TPU v7x, 512 devices: a whole 4x4x16 slice. The times are simulated.
512 devices in a mesh: dp: 4 (over x), kv: 64 (over z, y), tp: 2 (over core).
Axes of the slice: x: 4, y: 4, z: 16, core: 2. Of those that a mesh axis runs over, the one named last changes fastest.
Arguments:
- tokens: bfloat16 [512, 4096], P('dp', 'kv'), parts along dimension 0, may hold values from -16 to 16
- gain_mix: float32 [4096], P('kv'), may hold values from 0.1 to 1.9
- w_query: bfloat16 [4096, 2048], P('kv', 'tp'), may hold values from -0.09375 to 0.09375
- w_key: bfloat16 [4096, 2048], P('kv', 'tp'), may hold values from -0.09375 to 0.09375
- w_value: bfloat16 [4096, 2048], P('kv', 'tp'), may hold values from -0.09375 to 0.09375
- w_igate: bfloat16 [4096, 16], P('kv', 'tp'), may hold values from -0.09375 to 0.09375
- w_fgate: bfloat16 [4096, 16], P('kv', 'tp'), may hold values from -0.09375 to 0.09375
- bias_igate: float32 [16], P('tp'), may hold values from -1 to 1
- bias_fgate: float32 [16], P('tp'), may hold values from -1 to 4
- memory: float32 [512, 16, 128, 128], P(('dp', 'kv'), 'tp'), parts along dimension 0, may hold values from -0.8 to 0.8
- normalizer: float32 [512, 16, 128], P(('dp', 'kv'), 'tp'), parts along dimension 0, may hold values from -0.8 to 0.8
- stabilizer: float32 [512, 16], P(('dp', 'kv'), 'tp'), parts along dimension 0, may hold values from -1.5 to 1.5
- w_output: bfloat16 [2048, 4096], P('tp', 'kv'), may hold values from -0.125 to 0.125
- gain_mlp: float32 [4096], replicated, may hold values from 0.1 to 1.9
- w_gate: bfloat16 [4096, 11264], P(None, ('kv', 'tp')), may hold values from -0.09375 to 0.09375
- w_up: bfloat16 [4096, 11264], P(None, ('kv', 'tp')), may hold values from -0.09375 to 0.09375
- w_down: bfloat16 [11264, 4096], P(('kv', 'tp')), may hold values from -0.21875 to 0.21875
Outputs:
- mixed: bfloat16 [512, 4096], P('dp', ('kv', 'tp')), parts along dimension 0
- memory_next: float32 [512, 16, 128, 128], P(('dp', 'kv'), 'tp'), parts along dimension 0
- normalizer_next: float32 [512, 16, 128], P(('dp', 'kv'), 'tp'), parts along dimension 0
- stabilizer_next: float32 [512, 16], P(('dp', 'kv'), 'tp'), parts along dimension 0
There are 4 independent parts, one for each index of `dp`. A program takes and returns all parts, laid end to end along the dimension named above; an argument that names none is the same for every part. Nothing has to cross between parts.
All inputs are finite; a program needn't handle non-finite values.
Results may differ from a plain program's by a relative error of at most 0.014.
Values may be sent and summed in bfloat16 or wider, within the bound.
No kernel may reach another device: no remote copies, remote signals or barrier semaphores. Data moves between devices by JAX's collectives and lax.ppermute only.
A program may use at most 64 MiB of HBM per device.

v0:
```python
import jax
import jax.numpy as jnp
from jax import lax
from jax.sharding import Mesh
from jax.sharding import PartitionSpec as P

D = 4096
KV = ("kv_0", "kv_1")
DP_KV = ("dp", "kv_0", "kv_1")
KV_TP = ("kv_0", "kv_1", "tp")


epsilon = 1e-06


def gathered_by_axis(x, axes, dim):
    for axis in reversed(axes):
        x = lax.all_gather(x, axis, axis=dim, tiled=True)
    return x


def in_blocks(x, dim, peers):
    shape = x.shape
    tiles = x.reshape(*shape[:dim], peers, shape[dim] // peers, *shape[dim + 1 :])
    return jnp.moveaxis(tiles, dim, 0)


def summed_on_arrival(x, axis, dim):
    tiles = in_blocks(x, dim, lax.axis_size(axis))
    arrived = lax.all_to_all(tiles, axis, split_axis=0, concat_axis=0, tiled=True)
    return arrived.astype(jnp.float32).sum(axis=0)


def in_one_piece(arrays, axis, dim, along):
    columns = [a.reshape(*a.shape[:along], -1) for a in arrays]
    both = jnp.concatenate(columns, axis=along)
    filled, at, gathered = (summed_on_arrival(both, axis, dim), 0, [])
    for a, column in zip(arrays, columns):
        piece = filled[..., at : at + column.shape[along]]
        gathered.append(piece.reshape(*piece.shape[:along], *a.shape[along:]))
        at += column.shape[along]
    return tuple(gathered)


def joined_along(tiles, dim):
    shape = list(tiles.shape[1:])
    shape[dim] *= tiles.shape[0]
    return jnp.moveaxis(tiles, 0, dim).reshape(shape)


def sent_to_all(x, axis):
    copies = jnp.broadcast_to(x, (lax.axis_size(axis), *x.shape))
    return lax.all_to_all(copies, axis, split_axis=0, concat_axis=0, tiled=True)


def gathered_copies(x, axis, dim):
    return joined_along(sent_to_all(x, axis), dim)


def over_copies(x, axis):
    everything = sent_to_all(x, axis)
    return jnp.sum(everything.astype(jnp.float32), axis=0)


def swapped(x, axis, bit):
    return lax.ppermute(x, axis, [(i, i ^ 1 << bit) for i in range(lax.axis_size(axis))])


def cell_update(
    queries, key_proj, values, in_gate, log_forget, memory, normalizer, stabilizer, head_count
):
    batch_rows = queries.shape[0]
    query_heads = queries.astype(jnp.float32).reshape(batch_rows, head_count, -1)
    head_dim = query_heads.shape[2]
    key_heads = key_proj.astype(jnp.float32).reshape(
        batch_rows, head_count, head_dim
    ) * head_dim ** (-0.5)
    value_heads = values.astype(jnp.float32).reshape(batch_rows, head_count, head_dim)
    stab_next = jnp.maximum(stabilizer + log_forget, in_gate)
    keeping = jnp.exp(stabilizer + log_forget - stab_next)
    fresh_weight = jnp.exp(in_gate - stab_next)
    memory_next = (
        keeping[:, :, None, None] * memory
        + fresh_weight[:, :, None, None] * value_heads[:, :, :, None] * key_heads[:, :, None, :]
    )
    norm_next = keeping[:, :, None] * normalizer + fresh_weight[:, :, None] * key_heads
    numerator = jnp.einsum(
        "bhvk,bhk->bhv", memory_next, query_heads, precision=lax.Precision.HIGHEST
    )
    denominator = jnp.einsum("bhk,bhk->bh", norm_next, query_heads, precision=lax.Precision.HIGHEST)
    denominator = jnp.maximum(jnp.abs(denominator), jnp.exp(-stab_next))
    hidden = (numerator / denominator[:, :, None]).reshape(batch_rows, -1).astype(jnp.bfloat16)
    return (hidden, memory_next, norm_next, stab_next)


def mixer_block(residual, gain_mlp, w_gate, w_up, w_down, lower_rows, upper_rows):
    full_rows = gathered_by_axis(residual, KV, 1).astype(jnp.float32)
    scaling = lax.rsqrt(jnp.mean(full_rows * full_rows, axis=1, keepdims=True) + epsilon)
    normed = (full_rows * scaling * gain_mlp).astype(jnp.bfloat16)
    gate_act = jnp.dot(normed, w_gate, preferred_element_type=jnp.float32)
    up_act = jnp.dot(normed, w_up, preferred_element_type=jnp.float32)
    activated = (jax.nn.silu(gate_act) * up_act).astype(jnp.bfloat16)
    paired_units = lax.all_to_all(activated, "tp", split_axis=0, concat_axis=1, tiled=True)
    width = w_down.shape[0]
    down_terms = jnp.dot(paired_units[:, :width], lower_rows, preferred_element_type=jnp.float32)
    down_terms = down_terms + jnp.dot(
        paired_units[:, width:], upper_rows, preferred_element_type=jnp.float32
    )
    half_sums = summed_on_arrival(down_terms.astype(jnp.bfloat16), KV, 1)
    return lax.all_to_all(half_sums, "tp", split_axis=1, concat_axis=0, tiled=True)


def local(
    tokens,
    gain_mix,
    w_query,
    w_key,
    w_value,
    w_igate,
    w_fgate,
    bias_igate,
    bias_fgate,
    memory,
    normalizer,
    stabilizer,
    w_output,
    gain_mlp,
    w_gate,
    w_up,
    w_down,
):
    tok_float = tokens.astype(jnp.float32)
    scaled = (tok_float * gain_mix).astype(jnp.bfloat16)
    part_squares = jnp.sum(tok_float * tok_float, axis=1)
    query_part = jnp.dot(scaled, w_query, preferred_element_type=jnp.float32)
    key_part = jnp.dot(scaled, w_key, preferred_element_type=jnp.float32)
    value_part = jnp.dot(scaled, w_value, preferred_element_type=jnp.float32)
    igate_part = jnp.dot(scaled, w_igate, preferred_element_type=jnp.float32)
    fgate_part = jnp.dot(scaled, w_fgate, preferred_element_type=jnp.float32)
    query_sum, key_sum, value_sum, igate_sum, fgate_sum, own_squares = in_one_piece(
        (
            query_part.astype(jnp.bfloat16),
            key_part.astype(jnp.bfloat16),
            value_part.astype(jnp.bfloat16),
            igate_part.astype(jnp.bfloat16),
            fgate_part.astype(jnp.bfloat16),
            part_squares.astype(jnp.bfloat16),
        ),
        KV,
        0,
        1,
    )
    scaling = lax.rsqrt(own_squares / D + epsilon)[:, None]
    queries = (scaling * query_sum).astype(jnp.bfloat16)
    key_proj = (scaling * key_sum).astype(jnp.bfloat16)
    values = (scaling * value_sum).astype(jnp.bfloat16)
    in_gate = scaling * igate_sum + bias_igate
    log_forget = jax.nn.log_sigmoid(scaling * fgate_sum + bias_fgate)
    hidden, memory_next, norm_next, stab_next = cell_update(
        queries,
        key_proj,
        values,
        in_gate,
        log_forget,
        memory,
        normalizer,
        stabilizer,
        memory.shape[1],
    )
    branch_part = jnp.dot(
        gathered_copies(hidden, KV, 0), w_output, preferred_element_type=jnp.float32
    )
    branch = over_copies(branch_part.astype(jnp.bfloat16), "tp").astype(jnp.float32)
    residual = (tok_float + branch).astype(jnp.bfloat16)
    partner_rows = swapped(w_down, "tp", 0)
    first_core = lax.axis_index("tp") == 0
    lower_rows = jnp.where(first_core, w_down, partner_rows)
    upper_rows = jnp.where(first_core, partner_rows, w_down)
    mixed_terms = mixer_block(residual, gain_mlp, w_gate, w_up, w_down, lower_rows, upper_rows)
    columns = mixed_terms.shape[1]
    residual_own = lax.dynamic_slice_in_dim(residual, lax.axis_index("tp") * columns, columns, 1)
    mixed = (residual_own.astype(jnp.float32) + mixed_terms).astype(jnp.bfloat16)
    return (mixed, memory_next, norm_next, stab_next)


def solution(mesh):
    torus = Mesh(
        mesh.devices.reshape(mesh.shape["dp"], 16, 4, mesh.shape["tp"]),
        ("dp", "kv_0", "kv_1", "tp"),
    )
    in_specs = (
        P("dp", KV),
        P(KV),
        P(KV, "tp"),
        P(KV, "tp"),
        P(KV, "tp"),
        P(KV, "tp"),
        P(KV, "tp"),
        P("tp"),
        P("tp"),
        P(DP_KV, "tp", None, None),
        P(DP_KV, "tp", None),
        P(DP_KV, "tp"),
        P("tp", KV),
        P(),
        P(None, KV_TP),
        P(None, KV_TP),
        P(KV_TP, None),
    )
    out_specs = (P("dp", KV_TP), P(DP_KV, "tp", None, None), P(DP_KV, "tp", None), P(DP_KV, "tp"))
    return jax.shard_map(local, mesh=torus, in_specs=in_specs, out_specs=out_specs, check_vma=False)
```

profile of v0, /device:TPU:1, one launch (start us, length us, event | category | flops | bytes accessed | tf_op | source)
XLA Modules:
  0.0 260.0 jit_solution(14487738798445464333)
XLA Ops:
  7.3 0.8 fusion.14
  8.1 1.2 convolution_convert_fusion.2
  9.3 0.1 concatenate.14
  9.5 1.3 convolution_convert_fusion.1
  10.7 0.1 concatenate.15
  10.9 0.3 convolution_convert_fusion
  11.2 0.1 concatenate.16
  11.3 0.2 convolution_convert_fusion.5
  11.5 0.1 copy.38
  11.6 0.2 convolution_convert_fusion.4
  11.8 0.1 copy.39
  12.0 0.2 convert_element_type.111
  12.2 1.9 concatenate.19
  14.2 61.4 %all_to_all.58 = bf16[64,2,3089]{2,1,0:T(2,128)(2,1)S(1)} all-to-all(bf16[64,2,3089]{2,1,0:T(2,128)(2,1)S(1)} %concatenate.19), channel_id=1, replica_groups=mesh['dp'=4,'kv_0'=16,'kv_1'=4,'tp'=2] {'kv_0','kv_1'}, dimensions={0} | all-to-all | bytes 1581568 | tf_op jit(solution)/shard_map/all_to_all | solution.py:30
  75.6 0.7 convert_reduce_fusion.1
  76.3 0.2 fusion.30
  76.7 0.7 multiply_reduce_fusion
  77.4 0.4 multiply_add_fusion
  77.8 1.0 copy-done.1
  78.8 0.9 fusion.40
  79.8 0.1 broadcast_in_dim.4
  80.0 27.5 %all_to_all.59 = bf16[64,2,1024]{2,1,0:T(2,128)(2,1)S(1)} all-to-all(bf16[64,2,1024]{2,1,0:T(2,128)(2,1)S(1)} %broadcast_in_dim.4), channel_id=1, replica_groups=mesh['dp'=4,'kv_0'=16,'kv_1'=4,'tp'=2] {'kv_0','kv_1'}, dimensions={0} | all-to-all | bytes 524288 | tf_op jit(solution)/shard_map/all_to_all | solution.py:53
  107.5 0.1 reshape.87
  107.6 0.2 convolution_convert_fusion.3
  107.8 7.9 %all_to_all.60 = bf16[2,128,64]{1,2,0:T(8,128)(2,1)S(1)} all-to-all(bf16[2,128,64]{1,2,0:T(8,128)(2,1)S(1)} %broadcast_in_dim.5), channel_id=1, replica_groups=mesh['dp'=4,'kv_0'=16,'kv_1'=4,'tp'=2] {'tp'}, dimensions={0} | all-to-all | bytes 65536 | tf_op jit(solution)/shard_map/all_to_all | solution.py:53
  115.8 9.7 %all_gather.6 = bf16[128,256]{0,1:T(8,128)(2,1)} all-gather(bf16[128,64]{0,1:T(8,128)(2,1)S(1)} %fusion.15), channel_id=1, replica_groups=mesh['dp'=4,'kv_0'=16,'kv_1'=4,'tp'=2] {'kv_1'}, dimensions={1}, use_global_device_ids=true | all-gather | bytes 81920 | tf_op jit(solution)/shard_map/all_gather | solution.py:18
  125.5 5.1 %collective-permute-start = (bf16[88,4096]{1,0:T(8,128)(2,1)S(1)}, bf16[88,4096]{1,0:T(8,128)(2,1)S(1)}, u32[]{:S(2)}, u32[]{:S(2)}) collective-permute-start(bf16[88,4096]{1,0:T(8,128)(2,1)S(1)} %copy-done.2), channel_id=1, source_target_pairs={{0,1},{1,0},{2,3},{3,2},{4,5},{5,4},{6,7},{7,6},{8,9},{9,8},{10,11... | collective-permute-start | bytes 2162696 | tf_op jit(solution)/shard_map/ppermute | solution.py:66
  130.7 48.6 %all-gather.2.cloned.1.call-done = bf16[128,4096]{0,1:T(8,128)(2,1)} async-done(((bf16[128,256]{0,1:T(8,128)(2,1)}), bf16[128,4096]{0,1:T(8,128)(2,1)}) %all-gather.2.cloned.1.call-update) | async-done | bytes 1048592 | tf_op jit(solution)/shard_map/all_gather | solution.py:18
  179.3 1.9 fusion.1
  181.2 0.8 fusion.11
  182.0 0.3 copy-done.14
  182.3 0.8 fusion.4
  183.1 0.1 copy.41
  183.2 14.4 %all_to_all.61 = bf16[2,64,88]{2,1,0:T(8,128)(2,1)S(1)} all-to-all(bf16[2,64,88]{2,1,0:T(8,128)(2,1)S(1)} %bitcast.49), channel_id=1, replica_groups=mesh['dp'=4,'kv_0'=16,'kv_1'=4,'tp'=2] {'tp'}, dimensions={0} | all-to-all | bytes 45056 | tf_op jit(solution)/shard_map/all_to_all | solution.py:103
  197.8 0.3 fusion.5
  198.1 0.4 fusion
  198.5 1.1 reshape.88
  199.6 0.7 copy.64
  200.3 1.5 reshape.100
  201.8 11.0 %all-to-all-start.4 = ((bf16[64,2,2048]{2,1,0:T(2,128)(2,1)}), bf16[64,2,2048]{2,1,0:T(2,128)(2,1)S(1)}, u32[]{:S(2)}, u32[]{:S(2)}) async-start(bf16[64,2,2048]{2,1,0:T(2,128)(2,1)} %reshape.100), calls=%async_computation.4 | async-start | bytes 1048576 | tf_op jit(solution)/shard_map/all_to_all | solution.py:30
  212.9 31.0 %all-to-all-done.4 = bf16[64,2,2048]{2,1,0:T(2,128)(2,1)S(1)} async-done(((bf16[64,2,2048]{2,1,0:T(2,128)(2,1)}), bf16[64,2,2048]{2,1,0:T(2,128)(2,1)S(1)}, u32[]{:S(2)}, u32[]{:S(2)}) %all-to-all-start.4) | async-done | bytes 524320 | tf_op jit(solution)/shard_map/all_to_all | solution.py:30
  243.9 0.7 reshape.101
  244.5 0.2 convert_reduce_fusion
  244.8 0.1 reshape.102
  245.0 6.2 %all_to_all.62 = f32[2,1,2048]{2,1,0:T(1,128)S(1)} all-to-all(f32[2,1,2048]{2,1,0:T(1,128)S(1)} %reshape.102), channel_id=1, replica_groups=mesh['dp'=4,'kv_0'=16,'kv_1'=4,'tp'=2] {'tp'}, dimensions={0} | all-to-all | bytes 32768 | tf_op jit(solution)/shard_map/all_to_all | solution.py:110
  251.1 0.5 broadcast.50
  251.6 0.7 reduce.4
  252.5 0.6 add_convert_fusion
  (55 shorter events, 0.9 us)
Async XLA Ops:
  7.2 174.0 %copy-start = (bf16[4096,88]{0,1:T(8,128)(2,1)S(1)}, bf16[4096,88]{0,1:T(8,128)(2,1)}, u32[]{:S(2)}) copy-start(bf16[4096,88]{0,1:T(8,128)(2,1)} %param.31) | copy-start | bytes 2162692
  7.2 3.7 %copy-start.5 = (bf16[128,64]{0,1:T(8,128)(2,1)S(1)}, bf16[128,64]{0,1:T(8,128)(2,1)}, u32[]{:S(2)}) copy-start(bf16[128,64]{0,1:T(8,128)(2,1)} %param.17) | copy-start | bytes 49156
  7.2 3.7 %copy-start.10 = (f32[64]{0:T(128)S(1)}, f32[64]{0:T(128)}, u32[]{:S(2)}) copy-start(f32[64]{0:T(128)} %param.18) | copy-start | bytes 772
  7.2 3.7 %copy-start.7 = (bf16[64,1024]{1,0:T(8,128)(2,1)S(1)}, bf16[64,1024]{1,0:T(8,128)(2,1)}, u32[]{:S(2)}) copy-start(bf16[64,1024]{1,0:T(8,128)(2,1)} %param.21) | copy-start | bytes 393220
  7.2 172.1 %all-gather.2.cloned.1.call-start = ((), (), s32[]{:S(2)}) async-start(), calls=%async_computation.6 | async-start | bytes 1114112 | tf_op jit(solution)/shard_map/all_gather | solution.py:18
  9.5 1.9 copy-start.16
  9.5 2.2 copy-start.17
  14.1 62.5 %copy-start.11 = (f32[2,8]{1,0:T(2,128)S(1)}, f32[2,8]{1,0:T(2,128)}, u32[]{:S(2)}) copy-start(f32[2,8]{1,0:T(2,128)} %param.28) | copy-start | bytes 196
  14.1 62.4 %copy-start.12 = (f32[8]{0:T(128)S(1)}, f32[8]{0:T(128)}, u32[]{:S(2)}) copy-start(f32[8]{0:T(128)} %param.24) | copy-start | bytes 100
  14.1 62.4 %copy-start.13 = (f32[8]{0:T(128)S(1)}, f32[8]{0:T(128)}, u32[]{:S(2)}) copy-start(f32[8]{0:T(128)} %param.25) | copy-start | bytes 100
  14.1 62.6 %copy-start.9 = (f32[2,8,128]{2,1,0:T(8,128)S(1)}, f32[2,8,128]{2,1,0:T(8,128)}, u32[]{:S(2)}) copy-start(f32[2,8,128]{2,1,0:T(8,128)} %param.27) | copy-start | bytes 24580
  14.1 63.2 %copy-start.4 = (f32[2,8,128,128]{3,2,1,0:T(8,128)S(1)}, f32[2,8,128,128]{3,2,1,0:T(8,128)}, u32[]{:S(2)}) copy-start(f32[2,8,128,128]{3,2,1,0:T(8,128)} %param.26) | copy-start | bytes 3145732
  76.7 1.1 copy-start.8
  77.8 1.0 copy-start.1
  78.8 28.8 %copy-start.6 = (bf16[1024,64]{0,1:T(8,128)(2,1)S(1)}, bf16[1024,64]{0,1:T(8,128)(2,1)}, u32[]{:S(2)}) copy-start(bf16[1024,64]{0,1:T(8,128)(2,1)} %param.29) | copy-start | bytes 393220
  79.8 45.7 %copy-start.2 = (bf16[88,4096]{1,0:T(8,128)(2,1)S(1)}, bf16[88,4096]{1,0:T(8,128)(2,1)}, u32[]{:S(2)}) copy-start(bf16[88,4096]{1,0:T(8,128)(2,1)} %param.33) | copy-start | bytes 2162692
  107.6 73.6 %copy-start.15 = (f32[4096]{0:T(1024)S(1)}, f32[4096]{0:T(1024)}, u32[]{:S(2)}) copy-start(f32[4096]{0:T(1024)} %param.30) | copy-start | bytes 49156
  125.5 72.3 %collective-permute-start = (bf16[88,4096]{1,0:T(8,128)(2,1)S(1)}, bf16[88,4096]{1,0:T(8,128)(2,1)S(1)}, u32[]{:S(2)}, u32[]{:S(2)}) collective-permute-start(bf16[88,4096]{1,0:T(8,128)(2,1)S(1)} %copy-done.2), channel_id=1, source_target_pairs={{0,1},{1,0},{2,3},{3,2},{4,5},{5,4},{6,7},{7,6},{8,9},{9,8},{10,11... | collective-permute-start | bytes 2162696 | tf_op jit(solution)/shard_map/ppermute | solution.py:66
  179.3 1.9 copy-start.3
  181.2 1.1 copy-start.14
  201.8 42.0 %all-to-all-start.4 = ((bf16[64,2,2048]{2,1,0:T(2,128)(2,1)}), bf16[64,2,2048]{2,1,0:T(2,128)(2,1)S(1)}, u32[]{:S(2)}, u32[]{:S(2)}) async-start(bf16[64,2,2048]{2,1,0:T(2,128)(2,1)} %reshape.100), calls=%async_computation.4 | async-start | bytes 1048576 | tf_op jit(solution)/shard_map/all_to_all | solution.py:30
Sparse Core Ops, SparseCore 0:
  125.6 53.6 all-gather.1
where the time goes:
time: 261 us; the launch traced here: 260 us
  blocking collectives  127 us (49%)
  waiting for transfers between devices  79.6 us (30%)
  starting transfers between devices  16.2 us (6%)
  between operations  14.5 us (6%)
  local copies, waits for them, and re-layouts  9.46 us (4%)
  matrix products  6.63 us (3%)
  other arithmetic  6.45 us (2%)
    all_to_all x1, blocking collectives, summed_on_arrival(): lax.all_to_all(tiles, axis, split_axis=0, concat_axis=0, tiled=True)  61.4 us
    all_gather x1, waiting for transfers between devices, gathered_by_axis(): x = lax.all_gather(x, axis, axis=dim, tiled=True)  48.6 us
    all_to_all x2, blocking collectives, sent_to_all(): return lax.all_to_all(copies, axis, split_axis=0, concat_axis=0, tiled=True)  35.4 us
    all_to_all x1, waiting for transfers between devices, summed_on_arrival(): lax.all_to_all(tiles, axis, split_axis=0, concat_axis=0, tiled=True)  31 us
    all_to_all x1, blocking collectives, mixer_block(): lax.all_to_all(activated, 'tp', split_axis=0, concat_axis=1, tiled=True)  14.4 us
    all_to_all x1, starting transfers between devices, summed_on_arrival(): lax.all_to_all(tiles, axis, split_axis=0, concat_axis=0, tiled=True)  11 us
    all_gather x1, blocking collectives, gathered_by_axis(): x = lax.all_gather(x, axis, axis=dim, tiled=True)  9.71 us
    all_to_all x1, blocking collectives, mixer_block(): lax.all_to_all(half_sums, 'tp', split_axis=1, concat_axis=0, tiled=True)  6.17 us
  transfers between devices with their start and end apart: 3, of which 2 were waited for; matrix products, arithmetic and copies ran while one was open for 1% of the time, Pallas kernels for 0%

commit v1 on v0

v1 whole, which is shorter than its diff:
```python
import jax
import jax.numpy as jnp
from jax import lax
from jax.experimental import pallas as pl
from jax.experimental.pallas import tpu as pltpu
from jax.sharding import Mesh
from jax.sharding import PartitionSpec as P

D = 4096
KV = ("kv_0", "kv_1")
DP_KV = ("dp", "kv_0", "kv_1")
KV_TP = ("kv_0", "kv_1", "tp")
Z, Y = 16, 4
ROWS = 128
HALF = 32
BLOCK = Z * HALF
PADDED = BLOCK + 16
epsilon = 1e-06
f32 = jnp.float32
bf16 = jnp.bfloat16


def exchanged(x, axis):
    return lax.all_to_all(x, axis, split_axis=0, concat_axis=0, tiled=True)


def swapped(x):
    return lax.ppermute(x, "tp", [(0, 1), (1, 0)])


def contracted(a, b, dim_a, dim_b):
    return lax.dot_general(a, b, (((dim_a,), (dim_b,)), ((), ())), preferred_element_type=f32)


def natural_row(i):
    return 8 * ((i // 2) % Z) + 2 * (i // 32) + i % 2


def row_selection(transposed):
    a = lax.broadcasted_iota(jnp.int32, (ROWS, ROWS), 0)
    b = lax.broadcasted_iota(jnp.int32, (ROWS, ROWS), 1)
    if transposed:
        hit = natural_row(a) == b
    else:
        hit = a == natural_row(b)
    return jnp.where(hit, 1.0, 0.0).astype(bf16)


def high_low(x):
    lane = lax.broadcasted_iota(jnp.int32, x.shape, 1)
    high = x.astype(bf16)
    low = (x - high.astype(f32)).astype(bf16)
    return jnp.where(lane < 64, high.astype(f32), low.astype(f32)).astype(bf16)


def project_kernel(tok_ref, gain_ref, wq_ref, wk_ref, wv_ref, wi_ref, wf_ref, out_ref, tok_out_ref):
    perm = row_selection(False)
    tok = jnp.dot(tok_ref[...], perm, preferred_element_type=f32)
    tok_out_ref[...] = tok.astype(bf16)
    scaled = (tok * gain_ref[...]).astype(bf16)
    for n, ref in enumerate((wq_ref, wk_ref, wv_ref)):
        part = contracted(scaled, ref[...], 0, 0).astype(bf16)
        out_ref[:, :, 1024 * n : 1024 * (n + 1)] = part.reshape(Y, 32, 1024)
    gates = jnp.concatenate([wi_ref[...].astype(f32), wf_ref[...].astype(f32)], axis=0)
    rest = jnp.zeros((48, 64), f32)
    gates = jnp.concatenate([gates, rest, gates, rest], axis=0).astype(bf16)
    extra = contracted(scaled, gates, 0, 1)
    squares = tok * tok
    high = squares.astype(bf16)
    low = (squares - high.astype(f32)).astype(bf16)
    lane = lax.broadcasted_iota(jnp.int32, (64, 128), 1)
    ones = jnp.where(lane % 64 == 16, 1.0, 0.0).astype(bf16)
    extra = extra + contracted(high, ones, 0, 0) + contracted(low, ones, 0, 0)
    out_ref[:, :, 3072:] = high_low(extra).reshape(Y, 32, 128)


def sum_y_kernel(in_ref, out_ref):
    for n in range(3):
        cut = slice(1024 * n, 1024 * (n + 1))
        total = in_ref[0, :, cut].astype(f32)
        for y in range(1, Y):
            total = total + in_ref[y, :, cut].astype(f32)
        out_ref[:, :, cut] = total.astype(bf16).reshape(Z, 2, 1024)
    total = in_ref[0, :, 3072:].astype(f32)
    for y in range(1, Y):
        total = total + in_ref[y, :, 3072:].astype(f32)
    total = total + jnp.concatenate([total[:, 64:], total[:, :64]], axis=1)
    out_ref[:, :, 3072:] = high_low(total).reshape(Z, 2, 128)


def cell_update(queries, key_proj, values, in_gate, log_forget, memory, normalizer, stabilizer):
    batch_rows, head_count = stabilizer.shape
    query_heads = queries.astype(f32).reshape(batch_rows, head_count, -1)
    head_dim = query_heads.shape[2]
    key_heads = key_proj.astype(f32).reshape(batch_rows, head_count, head_dim) * head_dim ** (-0.5)
    value_heads = values.astype(f32).reshape(batch_rows, head_count, head_dim)
    stab_next = jnp.maximum(stabilizer + log_forget, in_gate)
    keeping = jnp.exp(stabilizer + log_forget - stab_next)
    fresh_weight = jnp.exp(in_gate - stab_next)
    memory_next = (
        keeping[:, :, None, None] * memory
        + fresh_weight[:, :, None, None] * value_heads[:, :, :, None] * key_heads[:, :, None, :]
    )
    norm_next = keeping[:, :, None] * normalizer + fresh_weight[:, :, None] * key_heads
    numerator = jnp.einsum(
        "bhvk,bhk->bhv", memory_next, query_heads, precision=lax.Precision.HIGHEST
    )
    denominator = jnp.einsum("bhk,bhk->bh", norm_next, query_heads, precision=lax.Precision.HIGHEST)
    denominator = jnp.maximum(jnp.abs(denominator), jnp.exp(-stab_next))
    hidden = (numerator / denominator[:, :, None]).astype(bf16)
    return (hidden, memory_next, norm_next, stab_next)


def gain_kernel(in_ref, gain_ref, out_ref):
    squares = jnp.zeros((HALF, ROWS), f32)
    for z in range(Z):
        x = in_ref[z].astype(f32)
        squares = squares + x * x
        scaled = (x * gain_ref[z]).astype(bf16)
        for y in range(Y):
            out_ref[y, HALF * z : HALF * (z + 1), :] = scaled
    total = jnp.sum(squares, axis=0, keepdims=True)
    high = total.astype(bf16).astype(f32)
    low = (total - high).astype(bf16).astype(f32)
    row = lax.broadcasted_iota(jnp.int32, (16, ROWS), 0)
    tail = jnp.where(row == 0, high, jnp.where(row == 1, low, 0.0)).astype(bf16)
    for y in range(Y):
        out_ref[y, BLOCK:, :] = tail


def mlp_kernel(core_ref, own_ref, other_ref, wg_ref, wu_ref, wd_ref, keep_ref, send_ref, x_ref):
    first = core_ref[0] == 0
    squares = jnp.zeros((16, ROWS), f32)
    for y in range(Y):
        squares = squares + own_ref[y, BLOCK:, :].astype(f32) + other_ref[y, BLOCK:, :].astype(f32)
    scaling = lax.rsqrt(jnp.sum(squares, axis=0, keepdims=True) / D + epsilon)

    for y in range(Y):
        for z in range(Z):
            at = 64 * (Y * z + y)
            own = own_ref[y, HALF * z : HALF * (z + 1), :]
            other = other_ref[y, HALF * z : HALF * (z + 1), :]
            x_ref[at : at + HALF, :] = jnp.where(first, own, other)
            x_ref[at + HALF : at + 64, :] = jnp.where(first, other, own)
    x = x_ref[...]
    gate = scaling * jnp.dot(wg_ref[...], x, preferred_element_type=f32)
    up = scaling * jnp.dot(wu_ref[...], x, preferred_element_type=f32)
    activated = (gate * jax.nn.sigmoid(gate) * up).astype(bf16)
    for m in range(2 * Z):
        part = contracted(wd_ref[:, 128 * m : 128 * (m + 1)], activated, 0, 0)
        z = m // 2
        for pair in range(2):
            y = 2 * (m % 2) + pair
            lower = part[64 * pair : 64 * pair + HALF]
            upper = part[64 * pair + HALF : 64 * pair + 64]
            keep_ref[y, HALF * z : HALF * (z + 1), :] = jnp.where(first, lower, upper)
            send_ref[y, HALF * z : HALF * (z + 1), :] = jnp.where(first, upper, lower).astype(bf16)


def finish_kernel(in_ref, res_ref, out_ref):
    total = res_ref[...].astype(f32)
    acc = in_ref[0].astype(f32)
    for z in range(1, Z):
        acc = acc + in_ref[z].astype(f32)
    mixed = (total + acc).astype(bf16)
    out_ref[...] = jnp.dot(mixed, row_selection(True), preferred_element_type=f32).astype(bf16)


def called(kernel, out_shape, flops=0, bytes_accessed=0, **kw):
    return pl.pallas_call(
        kernel,
        out_shape=out_shape,
        cost_estimate=pl.CostEstimate(
            flops=flops, bytes_accessed=bytes_accessed, transcendentals=0
        ),
        **kw,
    )


def local(
    tokens,
    gain_mix,
    w_query,
    w_key,
    w_value,
    w_igate,
    w_fgate,
    bias_igate,
    bias_fgate,
    memory,
    normalizer,
    stabilizer,
    w_output,
    gain_mlp,
    w_gate,
    w_up,
    w_down,
):
    core = lax.axis_index("tp")
    shape = jax.ShapeDtypeStruct
    gain_rows = jnp.broadcast_to(gain_mix[:, None], (64, ROWS))
    partials, tok = called(
        project_kernel,
        (shape((Y, 32, 3200), bf16), shape((64, ROWS), bf16)),
        flops=2 * 64 * 128 * 3200,
    )(tokens.T, gain_rows, w_query, w_key, w_value, w_igate.T, w_fgate.T)
    partials = exchanged(partials, "kv_1")
    partials = called(sum_y_kernel, shape((Z, 2, 3200), bf16), flops=10**6)(partials)
    partials = exchanged(partials, "kv_0")
    sums = partials.astype(f32).sum(axis=0)
    extra = sums[:, 3072:3136] + sums[:, 3136:]
    scaling = lax.rsqrt(extra[:, 16:17] / D + epsilon)
    queries = (scaling * sums[:, :1024]).astype(bf16)
    key_proj = (scaling * sums[:, 1024:2048]).astype(bf16)
    values = (scaling * sums[:, 2048:3072]).astype(bf16)
    in_gate = scaling * extra[:, :8] + bias_igate
    log_forget = jax.nn.log_sigmoid(scaling * extra[:, 8:16] + bias_fgate)
    hidden, memory_next, norm_next, stab_next = cell_update(
        queries, key_proj, values, in_gate, log_forget, memory, normalizer, stabilizer
    )
    hidden = jnp.broadcast_to(hidden.reshape(1, 16, 128), (Z, 16, 128))
    hidden = exchanged(hidden, "kv_0").reshape(32, 1024)
    hidden = exchanged(jnp.broadcast_to(hidden[None], (Y, 32, 1024)), "kv_1")
    hidden = hidden.reshape(ROWS, 1024)
    part = contracted(w_output.T, hidden, 1, 1).astype(bf16)
    arrived = swapped(lax.dynamic_slice_in_dim(part, HALF * (1 - core), HALF, 0))
    kept = lax.dynamic_slice_in_dim(part, HALF * core, HALF, 0)
    branch = kept.astype(f32) + arrived.astype(f32)
    tok_half = lax.dynamic_slice_in_dim(tok, HALF * core, HALF, 0)
    residual = (tok_half.astype(f32) + branch).astype(bf16)

    spread = exchanged(jnp.broadcast_to(residual[None], (Z, HALF, ROWS)), "kv_0")
    gain = lax.dynamic_slice(
        gain_mlp.reshape(Z, Y, 2, HALF), (0, lax.axis_index("kv_1"), core, 0), (Z, 1, 1, HALF)
    )
    gain = jnp.broadcast_to(gain.reshape(Z, HALF, 1), (Z, HALF, ROWS))
    spread = called(gain_kernel, shape((Y, PADDED, ROWS), bf16), flops=10**6)(spread, gain)
    spread = exchanged(spread, "kv_1")
    other = swapped(spread)
    keep, send = called(
        mlp_kernel,
        (shape((Y, BLOCK, ROWS), f32), shape((Y, BLOCK, ROWS), bf16)),
        flops=6 * 128 * 88 * 4096,
        in_specs=[pl.BlockSpec(memory_space=pltpu.SMEM)]
        + [pl.BlockSpec(memory_space=pltpu.VMEM)] * 5,
        scratch_shapes=[pltpu.VMEM((D, ROWS), bf16)],
    )(core.astype(jnp.int32).reshape(1), spread, other, w_gate.T, w_up.T, w_down)
    terms = (keep + swapped(send).astype(f32)).astype(bf16)
    terms = exchanged(terms, "kv_1").astype(f32).sum(axis=0).astype(bf16)
    terms = exchanged(terms.reshape(Z, HALF, ROWS), "kv_0")
    mixed = called(finish_kernel, shape((HALF, ROWS), bf16), flops=10**6)(terms, residual)
    return (mixed.T, memory_next, norm_next, stab_next)


def solution(mesh):
    torus = Mesh(
        mesh.devices.reshape(mesh.shape["dp"], Z, Y, mesh.shape["tp"]),
        ("dp", "kv_0", "kv_1", "tp"),
    )
    in_specs = (
        P("dp", KV),
        P(KV),
        P(KV, "tp"),
        P(KV, "tp"),
        P(KV, "tp"),
        P(KV, "tp"),
        P(KV, "tp"),
        P("tp"),
        P("tp"),
        P(DP_KV, "tp", None, None),
        P(DP_KV, "tp", None),
        P(DP_KV, "tp"),
        P("tp", KV),
        P(),
        P(None, KV_TP),
        P(None, KV_TP),
        P(KV_TP, None),
    )
    out_specs = (P("dp", KV_TP), P(DP_KV, "tp", None, None), P(DP_KV, "tp", None), P(DP_KV, "tp"))
    return jax.shard_map(local, mesh=torus, in_specs=in_specs, out_specs=out_specs, check_vma=False)
```

time: 261 us -> 173 us (0.66)
  waiting for transfers between devices: 79.6 us -> 21.6 us
  blocking collectives: 127 us -> 104 us
  between operations: 14.5 us -> 0.87 us
  Pallas kernels: 0 us -> 12.3 us
  matrix products: 6.63 us -> 1.12 us
  starting transfers between devices: 16.2 us -> 21.3 us
  local copies, waits for them, and re-layouts: 9.46 us -> 6.01 us
  other arithmetic: 6.45 us -> 3.18 us
    all_gather x1 -> x0, waiting for transfers between devices: 48.6 us -> none  [gathered_by_axis(): x = lax.all_gather(x, axis, axis=dim, tiled=True)]
    all_to_all x5 -> x6, blocking collectives: 117 us -> 104 us  [exchanged(): return lax.all_to_all(x, axis, split_axis=0, concat_axis=0, tiled=True)]
    all_to_all x1 -> x2, waiting for transfers between devices: 31 us -> 17.5 us  [exchanged(): return lax.all_to_all(x, axis, split_axis=0, concat_axis=0, tiled=True)]
    pallas_call x0 -> x5, Pallas kernels: none -> 12.3 us  [the longest x1 4.18 us: local(): called(mlp_kernel, (shape((Y, BLOCK, ROWS), f32), shape((Y, BLOCK, ROWS),...]
    all_gather x1 -> x0, blocking collectives: 9.71 us -> none  [gathered_by_axis(): x = lax.all_gather(x, axis, axis=dim, tiled=True)]
    ppermute x1 -> x3, starting transfers between devices: 5.14 us -> 14.2 us  [swapped(): return lax.ppermute(x, 'tp', [(0, 1), (1, 0)])]
    dot_general x10 -> x1, matrix products: 5.72 us -> 0.2 us  [contracted(): lax.dot_general(a, b, (((dim_a,), (dim_b,)), ((), ())), preferred_element...]
    ppermute x1 -> x3, waiting for transfers between devices: 0.01 us -> 4.07 us  [swapped(): return lax.ppermute(x, 'tp', [(0, 1), (1, 0)])]
  transfers between devices with their start and end apart: 3 -> 5, of which waited for: 2 -> 5; matrix products, arithmetic and copies ran while one was open for 1% -> 0% of each run, Pallas kernels for 0% -> 0%
where the time goes in v1:
time: 173 us; the launch traced here: 170 us
  blocking collectives  104 us (60%)
  waiting for transfers between devices  21.6 us (12%)
  starting transfers between devices  21.3 us (12%)
  Pallas kernels  12.3 us (7%)
  local copies, waits for them, and re-layouts  6.01 us (3%)
  other arithmetic  3.18 us (2%)
    all_to_all x6, blocking collectives, exchanged(): return lax.all_to_all(x, axis, split_axis=0, concat_axis=0, tiled=True)  104 us
    all_to_all x2, waiting for transfers between devices, exchanged(): return lax.all_to_all(x, axis, split_axis=0, concat_axis=0, tiled=True)  17.5 us
    ppermute x3, starting transfers between devices, swapped(): return lax.ppermute(x, 'tp', [(0, 1), (1, 0)])  14.2 us
    all_to_all x2, starting transfers between devices, exchanged(): return lax.all_to_all(x, axis, split_axis=0, concat_axis=0, tiled=True)  7.05 us
    pallas_call x1, Pallas kernels, local(): called(mlp_kernel, (shape((Y, BLOCK, ROWS), f32), shape((Y, BLOCK, ROWS),...  4.18 us
    ppermute x3, waiting for transfers between devices, swapped(): return lax.ppermute(x, 'tp', [(0, 1), (1, 0)])  4.07 us
  transfers between devices with their start and end apart: 5, of which 5 were waited for; matrix products, arithmetic and copies ran while one was open for 0% of the time, Pallas kernels for 0%

profile of v1, /device:TPU:1, one launch (start us, length us, event | category | flops | bytes accessed | tf_op | source)
XLA Modules:
  0.0 170.0 jit_solution(8978086495981493124)
XLA Ops:
  0.6 0.0 copy-start
  0.7 0.7 copy-done.12
  1.3 0.7 broadcast_in_dim.16.gain_ref
  2.0 2.6 %shard_map.192 = (bf16[4,32,3200]{2,1,0:T(8,128)(2,1)}, bf16[64,128]{1,0:T(8,128)(2,1)}) custom-call(bf16[64,128]{1,0:T(8,128)(2,1)} %bitcast.48, f32[64,128]{1,0:T(8,128)} %broadcast_in_dim.16.gain_ref, bf16[64,1024]{1,0:T(8,128)(2,1)} %wq_ref.1, bf16[64,1024]{1,0:T(8,128)(2,1)} %wk_ref.1, bf16[64,1024]{1,0:T(8,128)(2,1)} %wv_ref.1, ...), custom_call_target="tpu_custom_call" | custom-call | flops 52428800 | tf_op jit(solution)/shard_map/pallas_call | solution.py:202
  4.6 13.6 %all_to_all.40.in_ref = bf16[4,32,3200]{2,1,0:T(8,128)(2,1)} all-to-all(bf16[4,32,3200]{2,1,0:T(8,128)(2,1)} %get-tuple-element.9), channel_id=1, replica_groups=mesh['dp'=4,'kv_0'=16,'kv_1'=4,'tp'=2] {'kv_1'}, dimensions={0} | all-to-all | bytes 1638400 | tf_op jit(solution)/shard_map/all_to_all | solution.py:24
  18.2 2.1 %shard_map.193 = bf16[16,2,3200]{2,1,0:T(2,128)(2,1)} custom-call(bf16[4,32,3200]{2,1,0:T(8,128)(2,1)} %all_to_all.40.in_ref), custom_call_target="tpu_custom_call" | custom-call | flops 1000000 | tf_op jit(solution)/shard_map/pallas_call | solution.py:208
  20.2 30.2 %all_to_all.41 = bf16[16,2,3200]{2,1,0:T(2,128)(2,1)S(1)} all-to-all(bf16[16,2,3200]{2,1,0:T(2,128)(2,1)} %shard_map.193), channel_id=1, replica_groups=mesh['dp'=4,'kv_0'=16,'kv_1'=4,'tp'=2] {'kv_0'}, dimensions={0} | all-to-all | bytes 409600 | tf_op jit(solution)/shard_map/all_to_all | solution.py:24
  50.5 0.2 convert_reduce_fusion
  50.6 0.1 slice_add_fusion
  50.7 0.2 rsqrt_reduce_fusion
  50.9 0.1 fusion.3
  51.0 0.0 copy-start.11
  51.0 0.0 copy-start.13
  51.0 0.0 copy-start.14
  51.0 0.6 copy-done.11
  51.7 0.0 copy-done.14
  51.7 0.1 broadcast_multiply_fusion
  51.8 0.0 copy-start.9
  51.8 0.7 copy-done.9
  52.5 0.7 multiply_reduce_fusion
  53.2 0.4 multiply_add_fusion
  53.6 0.9 fusion.13
  54.5 0.1 fusion.6
  54.6 18.9 %all_to_all.42 = bf16[16,16,128]{2,1,0:T(8,128)(2,1)S(1)} all-to-all(bf16[16,16,128]{2,1,0:T(8,128)(2,1)S(1)} %broadcast_in_dim.18), channel_id=1, replica_groups=mesh['dp'=4,'kv_0'=16,'kv_1'=4,'tp'=2] {'kv_0'}, dimensions={0} | all-to-all | bytes 131072 | tf_op jit(solution)/shard_map/all_to_all | solution.py:24
  73.5 0.7 broadcast_in_dim.20
  74.3 3.4 %all-to-all-start.3 = ((bf16[4,32,1024]{2,1,0:T(8,128)(2,1)}), bf16[4,32,1024]{2,1,0:T(8,128)(2,1)S(1)}, u32[]{:S(2)}, u32[]{:S(2)}) async-start(bf16[4,32,1024]{2,1,0:T(8,128)(2,1)} %broadcast_in_dim.20), calls=%async_computation.3 | async-start | bytes 524288 | tf_op jit(solution)/shard_map/all_to_all | solution.py:24
  77.7 5.5 %all-to-all-done.3 = bf16[4,32,1024]{2,1,0:T(8,128)(2,1)S(1)} async-done(((bf16[4,32,1024]{2,1,0:T(8,128)(2,1)}), bf16[4,32,1024]{2,1,0:T(8,128)(2,1)S(1)}, u32[]{:S(2)}, u32[]{:S(2)}) %all-to-all-start.3) | async-done | bytes 262176 | tf_op jit(solution)/shard_map/all_to_all | solution.py:24
  83.2 0.2 convolution_convert_fusion
  83.4 7.2 %collective-permute-start = (bf16[32,128]{1,0:T(8,128)(2,1)S(1)}, bf16[32,128]{1,0:T(8,128)(2,1)S(1)}, u32[]{:S(2)}, u32[]{:S(2)}) collective-permute-start(bf16[32,128]{1,0:T(8,128)(2,1)S(1)} %dynamic-slice_bitcast_fusion), channel_id=1, source_target_pairs={{0,1},{1,0},{2,3},{3,2},{4,5},{5,4},{6,7},{7,6},{8,9},{9,8},{10,11... | collective-permute-start | bytes 24584 | tf_op jit(solution)/shard_map/ppermute | solution.py:28
  90.6 0.8 collective-permute-done
  91.4 0.7 broadcast_in_dim.21
  92.1 3.6 %all-to-all-start.4 = ((bf16[16,32,128]{2,1,0:T(8,128)(2,1)}), bf16[16,32,128]{2,1,0:T(8,128)(2,1)S(1)}, u32[]{:S(2)}, u32[]{:S(2)}) async-start(bf16[16,32,128]{2,1,0:T(8,128)(2,1)} %broadcast_in_dim.21), calls=%async_computation.4 | async-start | bytes 262144 | tf_op jit(solution)/shard_map/all_to_all | solution.py:24
  95.8 0.1 reshape.63
  95.9 12.1 %all-to-all-done.4.in_ref = bf16[16,32,128]{2,1,0:T(8,128)(2,1)S(1)} async-done(((bf16[16,32,128]{2,1,0:T(8,128)(2,1)}), bf16[16,32,128]{2,1,0:T(8,128)(2,1)S(1)}, u32[]{:S(2)}, u32[]{:S(2)}) %all-to-all-start.4) | async-done | bytes 131104 | tf_op jit(solution)/shard_map/all_to_all | solution.py:24
  108.0 0.8 broadcast_in_dim.23.gain_ref
  108.8 1.9 %shard_map.194 = bf16[4,528,128]{2,1,0:T(8,128)(2,1)} custom-call(bf16[16,32,128]{2,1,0:T(8,128)(2,1)} %copy-done.5, f32[16,32,128]{2,1,0:T(8,128)} %broadcast_in_dim.23.gain_ref), custom_call_target="tpu_custom_call" | custom-call | flops 1000000 | tf_op jit(solution)/shard_map/pallas_call | solution.py:237
  110.7 11.2 %all_to_all.43.own_ref = bf16[4,528,128]{2,1,0:T(8,128)(2,1)S(1)} all-to-all(bf16[4,528,128]{2,1,0:T(8,128)(2,1)} %shard_map.194), channel_id=1, replica_groups=mesh['dp'=4,'kv_0'=16,'kv_1'=4,'tp'=2] {'kv_1'}, dimensions={0} | all-to-all | bytes 1081344 | tf_op jit(solution)/shard_map/all_to_all | solution.py:24
  121.8 4.8 %collective-permute-start.1 = (bf16[4,528,128]{2,1,0:T(8,128)(2,1)S(1)}, bf16[4,528,128]{2,1,0:T(8,128)(2,1)S(1)}, u32[]{:S(2)}, u32[]{:S(2)}) collective-permute-start(bf16[4,528,128]{2,1,0:T(8,128)(2,1)S(1)} %all_to_all.43.own_ref), channel_id=1, source_target_pairs={{0,1},{1,0},{2,3},{3,2},{4,5},{5,4},{6,7},{7,6},{8,9},{9,8},{10,11... | collective-permute-start | bytes 1622024 | tf_op jit(solution)/shard_map/ppermute | solution.py:28
  126.6 1.5 collective-permute-done.1.other_ref
  128.2 0.8 copy-done.4
  129.0 4.2 %shard_map.195 = (f32[4,512,128]{2,1,0:T(8,128)}, bf16[4,512,128]{2,1,0:T(8,128)(2,1)}) custom-call(s32[1]{0:T(128)} %bitcast.core_ref, bf16[4,528,128]{2,1,0:T(8,128)(2,1)} %copy-done.2, bf16[4,528,128]{2,1,0:T(8,128)(2,1)} %copy-done.4, bf16[88,4096]{1,0:T(8,128)(2,1)} %bitcast.42, bf16[88,4096]{1,0:T(8,128)(2,1)} %bitcast.43, bf16[88,4096]{1,0:T(8,128)(2,1)} %wd_ref.1), custom_call_target="tpu_custom_call" | custom-call | flops 276824064 | tf_op jit(solution)/shard_map/pallas_call | solution.py:240
  133.2 2.3 %collective-permute-start.2 = (bf16[4,512,128]{2,1,0:T(8,128)(2,1)}, bf16[4,512,128]{2,1,0:T(8,128)(2,1)S(1)}, u32[]{:S(2)}, u32[]{:S(2)}) collective-permute-start(bf16[4,512,128]{2,1,0:T(8,128)(2,1)} %get-tuple-element.11), channel_id=1, source_target_pairs={{0,1},{1,0},{2,3},{3,2},{4,5},{5,4},{6,7},{7,6},{8,9},{9,8},{10,11... | collective-permute-start | bytes 1572872 | tf_op jit(solution)/shard_map/ppermute | solution.py:28
  135.4 1.7 %collective-permute-done.2 = bf16[4,512,128]{2,1,0:T(8,128)(2,1)S(1)} collective-permute-done((bf16[4,512,128]{2,1,0:T(8,128)(2,1)}, bf16[4,512,128]{2,1,0:T(8,128)(2,1)S(1)}, u32[]{:S(2)}, u32[]{:S(2)}) %collective-permute-start.2) | collective-permute-done | bytes 524320 | tf_op jit(solution)/shard_map/ppermute | solution.py:28
  137.2 1.3 add_convert_fusion
  138.5 11.6 %all_to_all.44 = bf16[4,512,128]{2,1,0:T(8,128)(2,1)S(1)} all-to-all(bf16[4,512,128]{2,1,0:T(8,128)(2,1)S(1)} %add_convert_fusion), channel_id=1, replica_groups=mesh['dp'=4,'kv_0'=16,'kv_1'=4,'tp'=2] {'kv_1'}, dimensions={0} | all-to-all | bytes 1048576 | tf_op jit(solution)/shard_map/all_to_all | solution.py:24
  150.1 0.1 reduce_sum.22
  150.2 18.1 %all_to_all.45.in_ref = bf16[16,32,128]{2,1,0:T(8,128)(2,1)} all-to-all(bf16[16,32,128]{2,1,0:T(8,128)(2,1)S(1)} %bitcast.44), channel_id=1, replica_groups=mesh['dp'=4,'kv_0'=16,'kv_1'=4,'tp'=2] {'kv_0'}, dimensions={0} | all-to-all | bytes 262144 | tf_op jit(solution)/shard_map/all_to_all | solution.py:24
  168.3 1.7 shard_map.196
  (28 shorter events, 0.2 us)
Async XLA Ops:
  0.6 82.5 %copy-start = (bf16[1024,64]{0,1:T(8,128)(2,1)S(1)}, bf16[1024,64]{0,1:T(8,128)(2,1)}, u32[]{:S(2)}) copy-start(bf16[1024,64]{0,1:T(8,128)(2,1)} %param.29) | copy-start | bytes 393220
  0.6 0.7 copy-start.12
  18.2 35.0 %copy-start.3 = (f32[2,8,128,128]{3,2,1,0:T(8,128)S(1)}, f32[2,8,128,128]{3,2,1,0:T(8,128)}, u32[]{:S(2)}) copy-start(f32[2,8,128,128]{3,2,1,0:T(8,128)} %param.26) | copy-start | bytes 3145732
  51.0 0.7 copy-start.11
  51.0 0.7 copy-start.13
  51.0 0.7 copy-start.14
  51.8 1.4 copy-start.8
  51.8 0.7 copy-start.9
  53.6 20.7 %copy-start.1 = (f32[2,8,128,128]{3,2,1,0:T(8,128)}, f32[2,8,128,128]{3,2,1,0:T(8,128)S(1)}, u32[]{:S(2)}) copy-start(f32[2,8,128,128]{3,2,1,0:T(8,128)S(1)} %multiply_add_fusion) | copy-start | bytes 3145732
  74.3 8.9 %all-to-all-start.3 = ((bf16[4,32,1024]{2,1,0:T(8,128)(2,1)}), bf16[4,32,1024]{2,1,0:T(8,128)(2,1)S(1)}, u32[]{:S(2)}, u32[]{:S(2)}) async-start(bf16[4,32,1024]{2,1,0:T(8,128)(2,1)} %broadcast_in_dim.20), calls=%async_computation.3 | async-start | bytes 524288 | tf_op jit(solution)/shard_map/all_to_all | solution.py:24
  83.4 8.0 %copy-start.10 = (bf16[64,128]{1,0:T(8,128)(2,1)S(1)}, bf16[64,128]{1,0:T(8,128)(2,1)}, u32[]{:S(2)}) copy-start(bf16[64,128]{1,0:T(8,128)(2,1)} %get-tuple-element.8) | copy-start | bytes 49156
  83.4 8.0 %collective-permute-start = (bf16[32,128]{1,0:T(8,128)(2,1)S(1)}, bf16[32,128]{1,0:T(8,128)(2,1)S(1)}, u32[]{:S(2)}, u32[]{:S(2)}) collective-permute-start(bf16[32,128]{1,0:T(8,128)(2,1)S(1)} %dynamic-slice_bitcast_fusion), channel_id=1, source_target_pairs={{0,1},{1,0},{2,3},{3,2},{4,5},{5,4},{6,7},{7,6},{8,9},{9,8},{10,11... | collective-permute-start | bytes 24584 | tf_op jit(solution)/shard_map/ppermute | solution.py:28
  91.4 0.7 copy-start.6
  92.1 3.7 %copy-start.7 = (f32[4096]{0:T(1024)S(1)}, f32[4096]{0:T(1024)}, u32[]{:S(2)}) copy-start(f32[4096]{0:T(1024)} %param.30) | copy-start | bytes 49156
  92.1 15.9 %all-to-all-start.4 = ((bf16[16,32,128]{2,1,0:T(8,128)(2,1)}), bf16[16,32,128]{2,1,0:T(8,128)(2,1)S(1)}, u32[]{:S(2)}, u32[]{:S(2)}) async-start(bf16[16,32,128]{2,1,0:T(8,128)(2,1)} %broadcast_in_dim.21), calls=%async_computation.4 | async-start | bytes 262144 | tf_op jit(solution)/shard_map/all_to_all | solution.py:24
  108.0 0.8 copy-start.5
  121.8 6.3 %copy-start.2 = (bf16[4,528,128]{2,1,0:T(8,128)(2,1)}, bf16[4,528,128]{2,1,0:T(8,128)(2,1)S(1)}, u32[]{:S(2)}) copy-start(bf16[4,528,128]{2,1,0:T(8,128)(2,1)S(1)} %all_to_all.43.own_ref) | copy-start | bytes 1622020
  121.8 6.3 %collective-permute-start.1 = (bf16[4,528,128]{2,1,0:T(8,128)(2,1)S(1)}, bf16[4,528,128]{2,1,0:T(8,128)(2,1)S(1)}, u32[]{:S(2)}, u32[]{:S(2)}) collective-permute-start(bf16[4,528,128]{2,1,0:T(8,128)(2,1)S(1)} %all_to_all.43.own_ref), channel_id=1, source_target_pairs={{0,1},{1,0},{2,3},{3,2},{4,5},{5,4},{6,7},{7,6},{8,9},{9,8},{10,11... | collective-permute-start | bytes 1622024 | tf_op jit(solution)/shard_map/ppermute | solution.py:28
  128.2 0.8 copy-start.4
  133.2 4.0 %collective-permute-start.2 = (bf16[4,512,128]{2,1,0:T(8,128)(2,1)}, bf16[4,512,128]{2,1,0:T(8,128)(2,1)S(1)}, u32[]{:S(2)}, u32[]{:S(2)}) collective-permute-start(bf16[4,512,128]{2,1,0:T(8,128)(2,1)} %get-tuple-element.11), channel_id=1, source_target_pairs={{0,1},{1,0},{2,3},{3,2},{4,5},{5,4},{6,7},{7,6},{8,9},{9,8},{10,11... | collective-permute-start | bytes 1572872 | tf_op jit(solution)/shard_map/ppermute | solution.py:28

commit v2 on v1

--- a/solution.py
+++ b/solution.py
@@ -53,14 +53,24 @@
     return jnp.where(lane < 64, high.astype(f32), low.astype(f32)).astype(bf16)
 
 
-def project_kernel(tok_ref, gain_ref, wq_ref, wk_ref, wv_ref, wi_ref, wf_ref, out_ref, tok_out_ref):
-    perm = row_selection(False)
-    tok = jnp.dot(tok_ref[...], perm, preferred_element_type=f32)
+def column_of(row, count, offset=0):
+    lane = lax.broadcasted_iota(jnp.int32, (count, row.shape[1]), 1)
+    at = lax.broadcasted_iota(jnp.int32, (count, row.shape[1]), 0)
+    return jnp.sum(jnp.where(lane == at + offset, row, 0.0), axis=1, keepdims=True)
+
+
+def project_kernel(
+    tok_ref, gain_ref, wi_ref, wf_ref, wq_ref, wk_ref, wv_ref, out_ref, tok_out_ref, w_ref, sems
+):
+    copies = [
+        pltpu.make_async_copy(ref, w_ref.at[n], sems.at[n])
+        for n, ref in enumerate((wq_ref, wk_ref, wv_ref))
+    ]
+    for copy in copies:
+        copy.start()
+    tok = jnp.dot(tok_ref[...], row_selection(False), preferred_element_type=f32)
     tok_out_ref[...] = tok.astype(bf16)
-    scaled = (tok * gain_ref[...]).astype(bf16)
-    for n, ref in enumerate((wq_ref, wk_ref, wv_ref)):
-        part = contracted(scaled, ref[...], 0, 0).astype(bf16)
-        out_ref[:, :, 1024 * n : 1024 * (n + 1)] = part.reshape(Y, 32, 1024)
+    scaled = (tok * column_of(gain_ref[...], 64)).astype(bf16)
     gates = jnp.concatenate([wi_ref[...].astype(f32), wf_ref[...].astype(f32)], axis=0)
     rest = jnp.zeros((48, 64), f32)
     gates = jnp.concatenate([gates, rest, gates, rest], axis=0).astype(bf16)
@@ -72,6 +82,10 @@
     ones = jnp.where(lane % 64 == 16, 1.0, 0.0).astype(bf16)
     extra = extra + contracted(high, ones, 0, 0) + contracted(low, ones, 0, 0)
     out_ref[:, :, 3072:] = high_low(extra).reshape(Y, 32, 128)
+    for n in range(3):
+        copies[n].wait()
+        part = contracted(scaled, w_ref[n], 0, 0).astype(bf16)
+        out_ref[:, :, 1024 * n : 1024 * (n + 1)] = part.reshape(Y, 32, 1024)
 
 
 def sum_y_kernel(in_ref, out_ref):
@@ -88,35 +102,90 @@
     out_ref[:, :, 3072:] = high_low(total).reshape(Z, 2, 128)
 
 
-def cell_update(queries, key_proj, values, in_gate, log_forget, memory, normalizer, stabilizer):
-    batch_rows, head_count = stabilizer.shape
-    query_heads = queries.astype(f32).reshape(batch_rows, head_count, -1)
-    head_dim = query_heads.shape[2]
-    key_heads = key_proj.astype(f32).reshape(batch_rows, head_count, head_dim) * head_dim ** (-0.5)
-    value_heads = values.astype(f32).reshape(batch_rows, head_count, head_dim)
-    stab_next = jnp.maximum(stabilizer + log_forget, in_gate)
-    keeping = jnp.exp(stabilizer + log_forget - stab_next)
-    fresh_weight = jnp.exp(in_gate - stab_next)
-    memory_next = (
-        keeping[:, :, None, None] * memory
-        + fresh_weight[:, :, None, None] * value_heads[:, :, :, None] * key_heads[:, :, None, :]
-    )
-    norm_next = keeping[:, :, None] * normalizer + fresh_weight[:, :, None] * key_heads
-    numerator = jnp.einsum(
-        "bhvk,bhk->bhv", memory_next, query_heads, precision=lax.Precision.HIGHEST
-    )
-    denominator = jnp.einsum("bhk,bhk->bh", norm_next, query_heads, precision=lax.Precision.HIGHEST)
+def by_head(x):
+    count = x.shape[1]
+    return jnp.concatenate(
+        [jnp.broadcast_to(x[0:1], (8, count)), jnp.broadcast_to(x[1:2], (8, count))], axis=0
+    )
+
+
+def picked(x, offset):
+    lane = lax.broadcasted_iota(jnp.int32, x.shape, 1)
+    head = lax.broadcasted_iota(jnp.int32, x.shape, 0) % 8
+    return jnp.sum(jnp.where(lane == head + offset, x, 0.0), axis=1, keepdims=True)
+
+
+def cell_kernel(
+    in_ref, bi_ref, bf_ref, mem_ref, norm_ref, stab_ref,
+    hid_ref, mem_out_ref, norm_out_ref, stab_out_ref, rows_ref,
+):
+    sums = in_ref[0].astype(f32)
+    for z in range(1, Z):
+        sums = sums + in_ref[z].astype(f32)
+    for n in range(3):
+        for j in range(2):
+            for h in range(8):
+                at = 1024 * n + 128 * h
+                rows_ref[n, 8 * j + h : 8 * j + h + 1, :] = sums[j : j + 1, at : at + 128]
+    extra = by_head(sums[:, 3072:3136] + sums[:, 3136:3200])
+    lane = lax.broadcasted_iota(jnp.int32, extra.shape, 1)
+    total = jnp.sum(jnp.where(lane == 16, extra, 0.0), axis=1, keepdims=True)
+    scaling = lax.rsqrt(total / D + epsilon)
+    in_gate = scaling * picked(extra, 0) + picked(jnp.broadcast_to(bi_ref[...], (16, 8)), 0)
+    forget = scaling * picked(extra, 8) + picked(jnp.broadcast_to(bf_ref[...], (16, 8)), 0)
+    log_forget = jnp.minimum(forget, 0.0) - jnp.log1p(jnp.exp(-jnp.abs(forget)))
+    kept = picked(by_head(stab_ref[...]), 0) + log_forget
+    stab_next = jnp.maximum(kept, in_gate)
+    keeping = jnp.exp(kept - stab_next)
+    fresh = jnp.exp(in_gate - stab_next)
+    queries = (scaling * rows_ref[0]).astype(bf16).astype(f32)
+    keys = (scaling * rows_ref[1]).astype(bf16).astype(f32) * 128 ** (-0.5)
+    values = (scaling * rows_ref[2]).astype(bf16).astype(f32)
+    norm_next = keeping * norm_ref[...] + fresh * keys
+    norm_out_ref[...] = norm_next
+    denominator = jnp.sum(norm_next * queries, axis=1, keepdims=True)
     denominator = jnp.maximum(jnp.abs(denominator), jnp.exp(-stab_next))
-    hidden = (numerator / denominator[:, :, None]).astype(bf16)
-    return (hidden, memory_next, norm_next, stab_next)
-
-
-def gain_kernel(in_ref, gain_ref, out_ref):
+    own = lax.broadcasted_iota(jnp.int32, (16, 8), 1)
+    head = lax.broadcasted_iota(jnp.int32, (16, 8), 0) % 8
+    spread = jnp.where(own == head, stab_next, 0.0)
+    stab_out_ref[0:1, :] = jnp.sum(spread[:8], axis=0, keepdims=True)
+    stab_out_ref[1:2, :] = jnp.sum(spread[8:], axis=0, keepdims=True)
+    added = jnp.concatenate([fresh * values, jnp.zeros((112, 128), f32)], axis=0).T
+    column = lax.broadcasted_iota(jnp.int32, (128, 128), 1)
+    numerator = jnp.zeros((128, 128), f32)
+    for i in range(16):
+        update = added[:, i : i + 1] * keys[i : i + 1, :]
+        mem_next = keeping[i : i + 1, :] * mem_ref[i] + update
+        mem_out_ref[i] = mem_next
+        read = jnp.sum(mem_next * queries[i : i + 1, :], axis=1, keepdims=True)
+        numerator = jnp.where(column == i, read, numerator)
+    hidden = (numerator.T[:16] / denominator).astype(bf16)
+    for z in range(Z):
+        hid_ref[z] = hidden
+
+
+def spread_kernel(in_ref, out_ref):
+    for n in range(out_ref.shape[0]):
+        out_ref[n] = in_ref[...]
+
+
+def residual_kernel(core_ref, part_ref, arrived_ref, tok_ref, out_ref, spread_ref):
+    first = core_ref[0] == 0
+    part = jnp.where(first, part_ref[:HALF], part_ref[HALF:]).astype(f32)
+    tok = jnp.where(first, tok_ref[:HALF], tok_ref[HALF:]).astype(f32)
+    residual = (tok + (part + arrived_ref[...].astype(f32))).astype(bf16)
+    out_ref[...] = residual
+    for z in range(Z):
+        spread_ref[z] = residual
+
+
+def gain_kernel(core_ref, in_ref, gain_ref, out_ref):
     squares = jnp.zeros((HALF, ROWS), f32)
     for z in range(Z):
         x = in_ref[z].astype(f32)
         squares = squares + x * x
-        scaled = (x * gain_ref[z]).astype(bf16)
+        gain = column_of(gain_ref[z : z + 1, :], HALF, core_ref[1])
+        scaled = (x * gain).astype(bf16)
         for y in range(Y):
             out_ref[y, HALF * z : HALF * (z + 1), :] = scaled
     total = jnp.sum(squares, axis=0, keepdims=True)
@@ -166,15 +235,19 @@
     out_ref[...] = jnp.dot(mixed, row_selection(True), preferred_element_type=f32).astype(bf16)
 
 
-def called(kernel, out_shape, flops=0, bytes_accessed=0, **kw):
+def called(kernel, out_shape, flops=0, grant=16, **kw):
     return pl.pallas_call(
         kernel,
         out_shape=out_shape,
-        cost_estimate=pl.CostEstimate(
-            flops=flops, bytes_accessed=bytes_accessed, transcendentals=0
-        ),
+        cost_estimate=pl.CostEstimate(flops=flops, bytes_accessed=10**6, transcendentals=0),
+        compiler_params=pltpu.CompilerParams(vmem_limit_bytes=grant * 2**20),
         **kw,
     )
+
+
+IN_VMEM = pl.BlockSpec(memory_space=pltpu.VMEM)
+IN_SMEM = pl.BlockSpec(memory_space=pltpu.SMEM)
+IN_HBM = pl.BlockSpec(memory_space=pltpu.HBM)
 
 
 def local(
@@ -197,59 +270,73 @@
     w_down,
 ):
     core = lax.axis_index("tp")
+    place = jnp.stack([core, 64 * lax.axis_index("kv_1") + HALF * core]).astype(jnp.int32)
     shape = jax.ShapeDtypeStruct
-    gain_rows = jnp.broadcast_to(gain_mix[:, None], (64, ROWS))
     partials, tok = called(
         project_kernel,
         (shape((Y, 32, 3200), bf16), shape((64, ROWS), bf16)),
         flops=2 * 64 * 128 * 3200,
-    )(tokens.T, gain_rows, w_query, w_key, w_value, w_igate.T, w_fgate.T)
+        in_specs=[IN_VMEM] * 4 + [IN_HBM] * 3,
+        scratch_shapes=[pltpu.VMEM((3, 64, 1024), bf16), pltpu.SemaphoreType.DMA((3,))],
+    )(tokens.T, gain_mix.reshape(1, 64), w_igate.T, w_fgate.T, w_query, w_key, w_value)
     partials = exchanged(partials, "kv_1")
     partials = called(sum_y_kernel, shape((Z, 2, 3200), bf16), flops=10**6)(partials)
     partials = exchanged(partials, "kv_0")
-    sums = partials.astype(f32).sum(axis=0)
-    extra = sums[:, 3072:3136] + sums[:, 3136:]
-    scaling = lax.rsqrt(extra[:, 16:17] / D + epsilon)
-    queries = (scaling * sums[:, :1024]).astype(bf16)
-    key_proj = (scaling * sums[:, 1024:2048]).astype(bf16)
-    values = (scaling * sums[:, 2048:3072]).astype(bf16)
-    in_gate = scaling * extra[:, :8] + bias_igate
-    log_forget = jax.nn.log_sigmoid(scaling * extra[:, 8:16] + bias_fgate)
-    hidden, memory_next, norm_next, stab_next = cell_update(
-        queries, key_proj, values, in_gate, log_forget, memory, normalizer, stabilizer
-    )
-    hidden = jnp.broadcast_to(hidden.reshape(1, 16, 128), (Z, 16, 128))
+    hidden, memory_next, norm_next, stab_next = called(
+        cell_kernel,
+        (
+            shape((Z, 16, 128), bf16),
+            shape((16, 128, 128), f32),
+            shape((16, 128), f32),
+            shape((2, 8), f32),
+        ),
+        flops=10**7,
+        scratch_shapes=[pltpu.VMEM((3, 16, 128), f32)],
+    )(
+        partials,
+        bias_igate.reshape(1, 8),
+        bias_fgate.reshape(1, 8),
+        memory.reshape(16, 128, 128),
+        normalizer.reshape(16, 128),
+        stabilizer,
+    )
     hidden = exchanged(hidden, "kv_0").reshape(32, 1024)
-    hidden = exchanged(jnp.broadcast_to(hidden[None], (Y, 32, 1024)), "kv_1")
-    hidden = hidden.reshape(ROWS, 1024)
+    hidden = called(spread_kernel, shape((Y, 32, 1024), bf16), flops=10**6)(hidden)
+    hidden = exchanged(hidden, "kv_1").reshape(ROWS, 1024)
     part = contracted(w_output.T, hidden, 1, 1).astype(bf16)
     arrived = swapped(lax.dynamic_slice_in_dim(part, HALF * (1 - core), HALF, 0))
-    kept = lax.dynamic_slice_in_dim(part, HALF * core, HALF, 0)
-    branch = kept.astype(f32) + arrived.astype(f32)
-    tok_half = lax.dynamic_slice_in_dim(tok, HALF * core, HALF, 0)
-    residual = (tok_half.astype(f32) + branch).astype(bf16)
-
-    spread = exchanged(jnp.broadcast_to(residual[None], (Z, HALF, ROWS)), "kv_0")
-    gain = lax.dynamic_slice(
-        gain_mlp.reshape(Z, Y, 2, HALF), (0, lax.axis_index("kv_1"), core, 0), (Z, 1, 1, HALF)
-    )
-    gain = jnp.broadcast_to(gain.reshape(Z, HALF, 1), (Z, HALF, ROWS))
-    spread = called(gain_kernel, shape((Y, PADDED, ROWS), bf16), flops=10**6)(spread, gain)
+    residual, spread = called(
+        residual_kernel,
+        (shape((HALF, ROWS), bf16), shape((Z, HALF, ROWS), bf16)),
+        flops=10**6,
+        in_specs=[IN_SMEM] + [IN_VMEM] * 3,
+    )(place, part, arrived, tok)
+    spread = exchanged(spread, "kv_0")
+    spread = called(
+        gain_kernel,
+        shape((Y, PADDED, ROWS), bf16),
+        flops=10**6,
+        in_specs=[IN_SMEM] + [IN_VMEM] * 2,
+    )(place, spread, gain_mlp.reshape(Z, 256))
     spread = exchanged(spread, "kv_1")
     other = swapped(spread)
     keep, send = called(
         mlp_kernel,
         (shape((Y, BLOCK, ROWS), f32), shape((Y, BLOCK, ROWS), bf16)),
         flops=6 * 128 * 88 * 4096,
-        in_specs=[pl.BlockSpec(memory_space=pltpu.SMEM)]
-        + [pl.BlockSpec(memory_space=pltpu.VMEM)] * 5,
+        in_specs=[IN_SMEM] + [IN_VMEM] * 5,
         scratch_shapes=[pltpu.VMEM((D, ROWS), bf16)],
-    )(core.astype(jnp.int32).reshape(1), spread, other, w_gate.T, w_up.T, w_down)
+    )(place, spread, other, w_gate.T, w_up.T, w_down)
     terms = (keep + swapped(send).astype(f32)).astype(bf16)
     terms = exchanged(terms, "kv_1").astype(f32).sum(axis=0).astype(bf16)
     terms = exchanged(terms.reshape(Z, HALF, ROWS), "kv_0")
     mixed = called(finish_kernel, shape((HALF, ROWS), bf16), flops=10**6)(terms, residual)
-    return (mixed.T, memory_next, norm_next, stab_next)
+    return (
+        mixed.T,
+        memory_next.reshape(2, 8, 128, 128),
+        norm_next.reshape(2, 8, 128),
+        stab_next,
+    )
 
 
 def solution(mesh):

time: 173 us -> 163 us (0.942)
  Pallas kernels: 12.3 us -> 9.34 us
  other arithmetic: 3.18 us -> 0.29 us
  blocking collectives: 104 us -> 102 us
    pallas_call x1 -> x4, Pallas kernels: 1.86 us -> 5.24 us  [the longest x1 2.64 us: local(): called(cell_kernel, (shape((Z, 16, 128), bf16), shape((16, 128, 128), f32...]
    broadcast_in_dim x6 -> x0, local copies, waits for them, and re-layouts: 2.97 us -> none  [the longest x1 0.84 us: local(): gain = jnp.broadcast_to(gain.reshape(Z, HALF, 1), (Z, HALF, ROWS))]
    pallas_call x1, Pallas kernels: 4.18 us -> 1.66 us  [local(): called(mlp_kernel, (shape((Y, BLOCK, ROWS), f32), shape((Y, BLOCK, ROWS),...]
    unnamed x30 -> x34, local copies, waits for them, and re-layouts: 2.88 us -> 4.85 us
    pallas_call x1, Pallas kernels: 2.06 us -> 0.15 us  [local(): called(sum_y_kernel, shape((Z, 2, 3200), bf16), flops=10 ** 6)(partials)]
where the time goes in v2:
time: 163 us; the launch traced here: 160 us
  blocking collectives  102 us (63%)
  waiting for transfers between devices  21.4 us (13%)
  starting transfers between devices  21.3 us (13%)
  Pallas kernels  9.34 us (6%)
  local copies, waits for them, and re-layouts  4.9 us (3%)
    all_to_all x6, blocking collectives, exchanged(): return lax.all_to_all(x, axis, split_axis=0, concat_axis=0, tiled=True)  102 us
    all_to_all x2, waiting for transfers between devices, exchanged(): return lax.all_to_all(x, axis, split_axis=0, concat_axis=0, tiled=True)  17.6 us
    ppermute x3, starting transfers between devices, swapped(): return lax.ppermute(x, 'tp', [(0, 1), (1, 0)])  14.2 us
    all_to_all x2, starting transfers between devices, exchanged(): return lax.all_to_all(x, axis, split_axis=0, concat_axis=0, tiled=True)  7.05 us
    unnamed x34, local copies, waits for them, and re-layouts  4.85 us
    ppermute x3, waiting for transfers between devices, swapped(): return lax.ppermute(x, 'tp', [(0, 1), (1, 0)])  3.78 us
  transfers between devices with their start and end apart: 5, of which 5 were waited for; matrix products, arithmetic and copies ran while one was open for 0% of the time, Pallas kernels for 0%

profile of v2, /device:TPU:1, one launch (start us, length us, event | category | flops | bytes accessed | tf_op | source)
XLA Modules:
  0.0 160.4 jit_solution(4564250207644239252)
XLA Ops:
  0.6 0.0 copy-start
  0.6 0.0 copy-start.11
  0.7 0.0 copy-start.10
  0.7 0.0 copy-start.15
  0.7 0.7 copy-done.11
  1.4 0.0 copy-done.10
  1.4 0.0 copy-done.15
  1.4 0.9 copy-done.5
  2.3 0.9 copy-done.6
  3.2 0.9 copy-done.7
  4.1 0.7 copy-done.8
  4.8 1.5 shard_map.192
  6.4 13.3 %all_to_all.40.in_ref = bf16[4,32,3200]{2,1,0:T(8,128)(2,1)S(1)} all-to-all(bf16[4,32,3200]{2,1,0:T(8,128)(2,1)S(1)} %get-tuple-element.14), channel_id=1, replica_groups=mesh['dp'=4,'kv_0'=16,'kv_1'=4,'tp'=2] {'kv_1'}, dimensions={0} | all-to-all | bytes 1638400 | tf_op jit(solution)/shard_map/all_to_all | solution.py:24
  19.7 0.1 shard_map.193
  19.8 0.0 copy-start.9
  19.8 0.0 copy-start.14
  19.8 30.2 %all_to_all.41.in_ref = bf16[16,2,3200]{2,1,0:T(2,128)(2,1)S(1)} all-to-all(bf16[16,2,3200]{2,1,0:T(2,128)(2,1)S(1)} %shard_map.193), channel_id=1, replica_groups=mesh['dp'=4,'kv_0'=16,'kv_1'=4,'tp'=2] {'kv_0'}, dimensions={0} | all-to-all | bytes 409600 | tf_op jit(solution)/shard_map/all_to_all | solution.py:24
  50.0 0.0 copy-done.1
  50.0 0.7 copy-done.12
  50.7 0.0 copy-done.13
  50.7 2.6 %shard_map.194 = (bf16[16,16,128]{2,1,0:T(8,128)(2,1)S(1)}, f32[16,128,128]{2,1,0:T(8,128)}, f32[16,128]{1,0:T(8,128)}, f32[2,8]{1,0:T(2,128)}) custom-call(bf16[16,2,3200]{2,1,0:T(2,128)(2,1)S(1)} %all_to_all.41.in_ref, f32[1,8]{1,0:T(1,128)S(1)} %bitcast.30, f32[1,8]{1,0:T(1,128)S(1)} %bitcast.31, f32[16,128,128]{2,1,0:T(8,128)S(1)} %bitcast.22, ...), custom_call_target="tpu_custom_call" | custom-call | flops 10000000 | bytes 1000000 | tf_op jit(solution)/shard_map/pallas_call | solution.py:285
  53.3 18.9 %all_to_all.42 = bf16[16,16,128]{2,1,0:T(8,128)(2,1)S(1)} all-to-all(bf16[16,16,128]{2,1,0:T(8,128)(2,1)S(1)} %get-tuple-element.15), channel_id=1, replica_groups=mesh['dp'=4,'kv_0'=16,'kv_1'=4,'tp'=2] {'kv_0'}, dimensions={0} | all-to-all | bytes 131072 | tf_op jit(solution)/shard_map/all_to_all | solution.py:24
  72.3 0.7 shard_map.195
  73.0 3.4 %all-to-all-start.3 = ((bf16[4,32,1024]{2,1,0:T(8,128)(2,1)}), bf16[4,32,1024]{2,1,0:T(8,128)(2,1)S(1)}, u32[]{:S(2)}, u32[]{:S(2)}) async-start(bf16[4,32,1024]{2,1,0:T(8,128)(2,1)} %shard_map.195), calls=%async_computation.3 | async-start | bytes 524288 | tf_op jit(solution)/shard_map/all_to_all | solution.py:24
  76.4 5.5 %all-to-all-done.3 = bf16[4,32,1024]{2,1,0:T(8,128)(2,1)S(1)} async-done(((bf16[4,32,1024]{2,1,0:T(8,128)(2,1)}), bf16[4,32,1024]{2,1,0:T(8,128)(2,1)S(1)}, u32[]{:S(2)}, u32[]{:S(2)}) %all-to-all-start.3) | async-done | bytes 262176 | tf_op jit(solution)/shard_map/all_to_all | solution.py:24
  81.9 0.0 copy-done
  81.9 0.2 convolution_convert_fusion
  82.1 7.2 %collective-permute-start = (bf16[32,128]{1,0:T(8,128)(2,1)S(1)}, bf16[32,128]{1,0:T(8,128)(2,1)S(1)}, u32[]{:S(2)}, u32[]{:S(2)}) collective-permute-start(bf16[32,128]{1,0:T(8,128)(2,1)S(1)} %dynamic-slice_bitcast_fusion), channel_id=1, source_target_pairs={{0,1},{1,0},{2,3},{3,2},{4,5},{5,4},{6,7},{7,6},{8,9},{9,8},{10,11... | collective-permute-start | bytes 24584 | tf_op jit(solution)/shard_map/ppermute | solution.py:28
  89.3 0.1 pad_add_fusion.core_ref
  89.4 0.7 collective-permute-done.arrived_ref
  90.1 1.2 shard_map.196
  91.3 3.6 %all-to-all-start.4 = ((bf16[16,32,128]{2,1,0:T(8,128)(2,1)}), bf16[16,32,128]{2,1,0:T(8,128)(2,1)S(1)}, u32[]{:S(2)}, u32[]{:S(2)}) async-start(bf16[16,32,128]{2,1,0:T(8,128)(2,1)} %get-tuple-element.17), calls=%async_computation.4 | async-start | bytes 262144 | tf_op jit(solution)/shard_map/all_to_all | solution.py:24
  95.0 0.0 copy-start.2
  95.0 0.0 copy-start.3
  95.0 12.2 %all-to-all-done.4.in_ref = bf16[16,32,128]{2,1,0:T(8,128)(2,1)S(1)} async-done(((bf16[16,32,128]{2,1,0:T(8,128)(2,1)}), bf16[16,32,128]{2,1,0:T(8,128)(2,1)S(1)}, u32[]{:S(2)}, u32[]{:S(2)}) %all-to-all-start.4) | async-done | bytes 131104 | tf_op jit(solution)/shard_map/all_to_all | solution.py:24
  107.2 0.7 shard_map.197
  107.8 10.1 %all_to_all.43.own_ref = bf16[4,528,128]{2,1,0:T(8,128)(2,1)S(1)} all-to-all(bf16[4,528,128]{2,1,0:T(8,128)(2,1)S(1)} %shard_map.197), channel_id=1, replica_groups=mesh['dp'=4,'kv_0'=16,'kv_1'=4,'tp'=2] {'kv_1'}, dimensions={0} | all-to-all | bytes 1081344 | tf_op jit(solution)/shard_map/all_to_all | solution.py:24
  118.0 4.8 %collective-permute-start.1 = (bf16[4,528,128]{2,1,0:T(8,128)(2,1)S(1)}, bf16[4,528,128]{2,1,0:T(8,128)(2,1)S(1)}, u32[]{:S(2)}, u32[]{:S(2)}) collective-permute-start(bf16[4,528,128]{2,1,0:T(8,128)(2,1)S(1)} %all_to_all.43.own_ref), channel_id=1, source_target_pairs={{0,1},{1,0},{2,3},{3,2},{4,5},{5,4},{6,7},{7,6},{8,9},{9,8},{10,11... | collective-permute-start | bytes 1622024 | tf_op jit(solution)/shard_map/ppermute | solution.py:28
  122.7 1.5 collective-permute-done.1.other_ref
  124.3 0.0 copy-done.4
  124.3 1.7 %shard_map.198 = (f32[4,512,128]{2,1,0:T(8,128)S(1)}, bf16[4,512,128]{2,1,0:T(8,128)(2,1)S(1)}) custom-call(s32[2]{0:T(128)S(1)} %pad_add_fusion.core_ref, bf16[4,528,128]{2,1,0:T(8,128)(2,1)S(1)} %all_to_all.43.own_ref, bf16[4,528,128]{2,1,0:T(8,128)(2,1)S(1)} %collective-permute-done.1.other_ref, bf16[88,4096]{1,0:T(8,128)(2,1)S(1)} %bitcast.23, ...), custom_call_target="tpu_custom_call" | custom-call | flops 276824064 | bytes 1000000 | tf_op jit(solution)/shard_map/pallas_call | solution.py:323
  125.9 2.3 %collective-permute-start.2 = (bf16[4,512,128]{2,1,0:T(8,128)(2,1)S(1)}, bf16[4,512,128]{2,1,0:T(8,128)(2,1)S(1)}, u32[]{:S(2)}, u32[]{:S(2)}) collective-permute-start(bf16[4,512,128]{2,1,0:T(8,128)(2,1)S(1)} %get-tuple-element.19), channel_id=1, source_target_pairs={{0,1},{1,0},{2,3},{3,2},{4,5},{5,4},{6,7},{7,6},{8,9},{9,8},{10,11... | collective-permute-start | bytes 1572872 | tf_op jit(solution)/shard_map/ppermute | solution.py:28
  128.2 1.5 collective-permute-done.2
  129.8 0.1 add_convert_fusion
  129.9 11.6 %all_to_all.44 = bf16[4,512,128]{2,1,0:T(8,128)(2,1)S(1)} all-to-all(bf16[4,512,128]{2,1,0:T(8,128)(2,1)S(1)} %add_convert_fusion), channel_id=1, replica_groups=mesh['dp'=4,'kv_0'=16,'kv_1'=4,'tp'=2] {'kv_1'}, dimensions={0} | all-to-all | bytes 1048576 | tf_op jit(solution)/shard_map/all_to_all | solution.py:24
  141.5 0.1 reduce_sum.12
  141.6 18.0 %all_to_all.45.in_ref = bf16[16,32,128]{2,1,0:T(8,128)(2,1)S(1)} all-to-all(bf16[16,32,128]{2,1,0:T(8,128)(2,1)S(1)} %bitcast.34), channel_id=1, replica_groups=mesh['dp'=4,'kv_0'=16,'kv_1'=4,'tp'=2] {'kv_0'}, dimensions={0} | all-to-all | bytes 262144 | tf_op jit(solution)/shard_map/all_to_all | solution.py:24
  159.6 0.8 shard_map.199
  (17 shorter events, 0.1 us)
Async XLA Ops:
  0.6 81.2 %copy-start = (bf16[1024,64]{0,1:T(8,128)(2,1)S(1)}, bf16[1024,64]{0,1:T(8,128)(2,1)}, u32[]{:S(2)}) copy-start(bf16[1024,64]{0,1:T(8,128)(2,1)} %param.29) | copy-start | bytes 393220
  0.6 0.7 copy-start.11
  0.7 0.7 copy-start.10
  0.7 0.7 copy-start.15
  1.4 0.9 copy-start.5
  2.3 0.9 copy-start.6
  3.2 0.9 copy-start.7
  4.1 0.7 copy-start.8
  19.7 30.4 %copy-start.1 = (f32[2,8,128,128]{3,2,1,0:T(8,128)S(1)}, f32[2,8,128,128]{3,2,1,0:T(8,128)}, u32[]{:S(2)}) copy-start(f32[2,8,128,128]{3,2,1,0:T(8,128)} %param.26) | copy-start | bytes 3145732
  19.8 30.2 %copy-start.9 = (f32[2,8,128]{2,1,0:T(8,128)S(1)}, f32[2,8,128]{2,1,0:T(8,128)}, u32[]{:S(2)}) copy-start(f32[2,8,128]{2,1,0:T(8,128)} %param.27) | copy-start | bytes 24580
  19.8 30.2 %copy-start.14 = (f32[8]{0:T(128)S(1)}, f32[8]{0:T(128)}, u32[]{:S(2)}) copy-start(f32[8]{0:T(128)} %param.25) | copy-start | bytes 100
  50.0 0.7 copy-start.12
  50.0 0.7 copy-start.13
  73.0 8.9 %all-to-all-start.3 = ((bf16[4,32,1024]{2,1,0:T(8,128)(2,1)}), bf16[4,32,1024]{2,1,0:T(8,128)(2,1)S(1)}, u32[]{:S(2)}, u32[]{:S(2)}) async-start(bf16[4,32,1024]{2,1,0:T(8,128)(2,1)} %shard_map.195), calls=%async_computation.3 | async-start | bytes 524288 | tf_op jit(solution)/shard_map/all_to_all | solution.py:24
  81.9 42.4 %copy-start.4 = (bf16[88,4096]{1,0:T(8,128)(2,1)S(1)}, bf16[88,4096]{1,0:T(8,128)(2,1)}, u32[]{:S(2)}) copy-start(bf16[88,4096]{1,0:T(8,128)(2,1)} %wd_ref.1) | copy-start | bytes 2162692
  82.1 8.0 %collective-permute-start = (bf16[32,128]{1,0:T(8,128)(2,1)S(1)}, bf16[32,128]{1,0:T(8,128)(2,1)S(1)}, u32[]{:S(2)}, u32[]{:S(2)}) collective-permute-start(bf16[32,128]{1,0:T(8,128)(2,1)S(1)} %dynamic-slice_bitcast_fusion), channel_id=1, source_target_pairs={{0,1},{1,0},{2,3},{3,2},{4,5},{5,4},{6,7},{7,6},{8,9},{9,8},{10,11... | collective-permute-start | bytes 24584 | tf_op jit(solution)/shard_map/ppermute | solution.py:28
  91.3 3.7 %copy-start.16 = (f32[4096]{0:T(1024)S(1)}, f32[4096]{0:T(1024)}, u32[]{:S(2)}) copy-start(f32[4096]{0:T(1024)} %param.30) | copy-start | bytes 49156
  91.3 15.9 %all-to-all-start.4 = ((bf16[16,32,128]{2,1,0:T(8,128)(2,1)}), bf16[16,32,128]{2,1,0:T(8,128)(2,1)S(1)}, u32[]{:S(2)}, u32[]{:S(2)}) async-start(bf16[16,32,128]{2,1,0:T(8,128)(2,1)} %get-tuple-element.17), calls=%async_computation.4 | async-start | bytes 262144 | tf_op jit(solution)/shard_map/all_to_all | solution.py:24
  95.0 29.3 %copy-start.2 = (bf16[4096,88]{0,1:T(8,128)(2,1)S(1)}, bf16[4096,88]{0,1:T(8,128)(2,1)}, u32[]{:S(2)}) copy-start(bf16[4096,88]{0,1:T(8,128)(2,1)} %param.31) | copy-start | bytes 2162692
  95.0 29.3 %copy-start.3 = (bf16[4096,88]{0,1:T(8,128)(2,1)S(1)}, bf16[4096,88]{0,1:T(8,128)(2,1)}, u32[]{:S(2)}) copy-start(bf16[4096,88]{0,1:T(8,128)(2,1)} %param.32) | copy-start | bytes 2162692
  118.0 6.3 %collective-permute-start.1 = (bf16[4,528,128]{2,1,0:T(8,128)(2,1)S(1)}, bf16[4,528,128]{2,1,0:T(8,128)(2,1)S(1)}, u32[]{:S(2)}, u32[]{:S(2)}) collective-permute-start(bf16[4,528,128]{2,1,0:T(8,128)(2,1)S(1)} %all_to_all.43.own_ref), channel_id=1, source_target_pairs={{0,1},{1,0},{2,3},{3,2},{4,5},{5,4},{6,7},{7,6},{8,9},{9,8},{10,11... | collective-permute-start | bytes 1622024 | tf_op jit(solution)/shard_map/ppermute | solution.py:28
  125.9 3.8 %collective-permute-start.2 = (bf16[4,512,128]{2,1,0:T(8,128)(2,1)S(1)}, bf16[4,512,128]{2,1,0:T(8,128)(2,1)S(1)}, u32[]{:S(2)}, u32[]{:S(2)}) collective-permute-start(bf16[4,512,128]{2,1,0:T(8,128)(2,1)S(1)} %get-tuple-element.19), channel_id=1, source_target_pairs={{0,1},{1,0},{2,3},{3,2},{4,5},{5,4},{6,7},{7,6},{8,9},{9,8},{10,11... | collective-permute-start | bytes 1572872 | tf_op jit(solution)/shard_map/ppermute | solution.py:28
